TPU v7x, 32 devices: a whole 2x2x4 slice. The times are simulated.
32 devices in a mesh: ra: 4 (over z), cb: 8 (over y, x, core).
Axes of the slice: x: 2, y: 2, z: 4, core: 2. Of those that a mesh axis runs over, the one named last changes fastest.
Arguments:
- tokens: bfloat16 [512, 3072], P(None, 'ra'), may hold values from -14 to 14
- norm_gain: float32 [2, 3072], P(None, 'ra'), may hold values from 0.1 to 1.9
- gate_weight: float32 [2, 3072, 8448], P(None, 'ra', 'cb'), may hold values from -0.109375 to 0.109375
- gate_scale: float32 [2, 8448], P(None, 'cb'), may hold values from 0.5 to 2
- value_weight: float32 [2, 3072, 8448], P(None, 'ra', 'cb'), may hold values from -0.109375 to 0.109375
- value_scale: float32 [2, 8448], P(None, 'cb'), may hold values from 0.5 to 2
- gate_conv: float32 [2, 3, 8448], P(None, None, 'cb'), may hold values from -3.5 to 3.5
- value_conv: float32 [2, 3, 8448], P(None, None, 'cb'), may hold values from -3.5 to 3.5
- gate_bias: float32 [2, 8448], P(None, 'cb'), may hold values from -3 to 3
- value_bias: float32 [2, 8448], P(None, 'cb'), may hold values from -3 to 3
- down_weight: float32 [2, 8448, 3072], P(None, 'cb', 'ra'), may hold values from -0.0625 to 0.0625
- down_scale: float32 [2, 3072], P(None, 'ra'), may hold values from 0.5 to 2
Outputs:
- stream_out: bfloat16 [512, 3072], P(None, 'ra')
All inputs are finite; a program needn't handle non-finite values.
Results may differ from a plain program's by a relative error of at most 0.039.
Values may be sent and summed in bfloat16 or wider, within the bound.
A program may use at most 64 MiB of HBM per device.

v0:
```python
import functools
import jax
import jax.numpy as jnp
from jax import lax
from jax.experimental import pallas as pl
from jax.experimental.pallas import tpu as pltpu
from jax.sharding import PartitionSpec as P

SEQ_LEN = 8
EPSILON = 1e-06
RESIDUAL_KEEP = 0.5
MESH = pl.DeviceIdType.MESH
LANES = 128


def kernel(
    cfg,
    tokens_ref,
    gain_ref,
    gw_ref,
    gs_ref,
    vw_ref,
    vs_ref,
    gc_ref,
    vc_ref,
    gb_ref,
    vb_ref,
    dw_ref,
    ds_ref,
    out_ref,
    stage_g,
    stage_v,
    stage_d,
    wc,
    wd,
    par,
    xs,
    own,
    pin,
    pout,
    hid,
    ro,
    ri,
    w_sem,
    ps,
    pr,
    hs,
    hr,
    rs_s,
    rs_r,
    ag_s,
    ag_r,
):
    R, N, L, n, m, D, F = cfg
    Dl = tokens_ref.shape[1]
    rows = 2 * m
    own_rows = rows // N
    taps = gc_ref.shape[0]
    full = F // LANES * LANES
    rest = F - full
    wide = full + LANES
    sq_lane = 2 * rest
    S = max(n, 2 * R)
    z = lax.axis_index("ra")
    me = lax.axis_index("cb")

    def weight_copy(l, k):
        src, dst = ((gw_ref, stage_g), (vw_ref, stage_v), (dw_ref, stage_d))[k]
        return pltpu.make_async_copy(src.at[l], dst, w_sem.at[k])

    for k in range(3):
        weight_copy(0, k).start()

    barrier = pltpu.get_barrier_semaphore()
    for k in range(1, N):
        pl.semaphore_signal(
            barrier, inc=1, device_id={"cb": lax.rem(me + k, N)}, device_id_type=MESH
        )

    @pl.when(z > 0)
    def _():
        pl.semaphore_signal(barrier, inc=1, device_id={"ra": z - 1}, device_id_type=MESH)

    @pl.when(z < R - 1)
    def _():
        pl.semaphore_signal(barrier, inc=1, device_id={"ra": z + 1}, device_id_type=MESH)

    for i in range(n):
        block = tokens_ref[i * rows : (i + 1) * rows, :].astype(jnp.float32)
        xs[i] = block.reshape(N, own_rows, Dl).astype(jnp.bfloat16)

    par[...] = jnp.zeros_like(par)
    for l in range(L):
        par[l, 0:1, 0:F] = gs_ref[l : l + 1, :]
        par[l, 1:2, 0:F] = vs_ref[l : l + 1, :]
        par[l, 2:3, 0:F] = gb_ref[l : l + 1, :]
        par[l, 3:4, 0:F] = vb_ref[l : l + 1, :]
        for k in range(taps):
            par[l, 4 + k : 5 + k, 0:F] = gc_ref[k, l : l + 1, :]
            par[l, 4 + taps + k : 5 + taps + k, 0:F] = vc_ref[k, l : l + 1, :]

    def cast_rows(dst, l, first, src, start, count, step):
        def move(b, carry):
            to = pl.ds(pl.multiple_of(first + b * step, step), step)
            at = pl.ds(pl.multiple_of(start + b * step, step), step)
            dst[l, to, :] = src[at, :].astype(jnp.bfloat16)
            return carry

        lax.fori_loop(0, count // step, move, 0)

    def cast_up(l):
        weight_copy(l, 0).wait()
        cast_rows(wc, l, 0, stage_g, 0, full, 64)
        cast_rows(wc, l, 2 * full, stage_g, full, rest, 32)
        weight_copy(l, 1).wait()
        cast_rows(wc, l, full, stage_v, 0, full, 64)
        cast_rows(wc, l, 2 * full + rest, stage_v, full, rest, 32)
        wc[l, 2 * F :, :] = jnp.zeros((wc.shape[1] - 2 * F, Dl), jnp.bfloat16)
        if l + 1 < L:
            weight_copy(l + 1, 0).start()
            weight_copy(l + 1, 1).start()

    def cast_down(l):
        weight_copy(l, 2).wait()
        cast_rows(wd, l, 0, stage_d, 0, F, 32)
        wd[l, F:wide, :] = jnp.zeros((wide - F, Dl), jnp.bfloat16)
        if l + 1 < L:
            weight_copy(l + 1, 2).start()

    cast_up(0)

    expected = N - 1 + jnp.where(z > 0, 1, 0) + jnp.where(z < R - 1, 1, 0)
    pl.semaphore_wait(barrier, expected)

    def when_item(g, fn):
        layer = lax.div(g, S)
        i = lax.rem(g, S)

        @pl.when((g >= 0) & (g < L * S) & (i < n))
        def _():
            fn(layer, i, layer * n + i)

    def part_copy(q, d, target):
        return pltpu.make_async_remote_copy(
            src_ref=pout.at[q, d],
            dst_ref=pin.at[q, d],
            send_sem=ps.at[q, d],
            recv_sem=pr.at[q, d],
            device_id={"ra": target},
            device_id_type=MESH,
        )

    def hid_copy(q, d, target):
        return pltpu.make_async_remote_copy(
            src_ref=hid.at[q, d],
            dst_ref=hid.at[q, d],
            send_sem=hs.at[q, d],
            recv_sem=hr.at[q, d],
            device_id={"ra": target},
            device_id_type=MESH,
        )

    row_in_seq = lax.rem(lax.broadcasted_iota(jnp.int32, (m, wide), 0), SEQ_LEN)
    lane = lax.broadcasted_iota(jnp.int32, (m, LANES), 1)

    def conv(values, l, first):
        total = values * par[l, first + taps - 1 : first + taps, :]
        for back in range(1, taps):
            moved = jnp.where(row_in_seq >= back, pltpu.roll(values, back, 0), 0.0)
            total = total + moved * par[l, first + taps - 1 - back : first + taps - back, :]
        return total

    def finish(l, q, d, main_g, main_v, tail):
        squares = jnp.sum(
            jnp.where((lane == sq_lane) | (lane == sq_lane + 1), tail, 0.0),
            axis=1,
            keepdims=True,
        )
        inverse = lax.rsqrt(squares / D + EPSILON)
        gate = jnp.concatenate([main_g, tail], axis=1)
        value = jnp.concatenate([main_v, pltpu.roll(tail, LANES - rest, 1)], axis=1)
        gate = gate * inverse * par[l, 0:1, :]
        value = value * inverse * par[l, 1:2, :]
        gate = par[l, 2:3, :] + conv(gate, l, 4)
        value = par[l, 3:4, :] + conv(value, l, 4 + taps)
        hid[q, d] = (gate / (1.0 + jnp.exp(-gate)) * value).astype(jnp.bfloat16)

    def chain(d, l, q):
        first = (z == 0) if d == 0 else (z == R - 1)
        last = (z == R - 1) if d == 0 else (z == 0)
        ahead = z + 1 if d == 0 else z - 1
        behind = z - 1 if d == 0 else z + 1

        def send(main_g, main_v, tail):
            squares = jnp.sum(
                jnp.where((lane == sq_lane) | (lane == sq_lane + 1), tail, 0.0),
                axis=1,
                keepdims=True,
            )
            high = squares.astype(jnp.bfloat16).astype(jnp.float32)
            tail = jnp.where(
                lane == sq_lane,
                high,
                jnp.where(lane == sq_lane + 1, squares - high, tail),
            )
            pout[q, d, :, 0:full] = main_g.astype(jnp.bfloat16)
            pout[q, d, :, full : 2 * full] = main_v.astype(jnp.bfloat16)
            pout[q, d, :, 2 * full : 2 * full + LANES] = tail.astype(jnp.bfloat16)
            part_copy(q, d, ahead).start()

        def pieces(ref):
            return (
                ref[q, d, :, 0:full].astype(jnp.float32),
                ref[q, d, :, full : 2 * full].astype(jnp.float32),
                ref[q, d, :, 2 * full : 2 * full + LANES].astype(jnp.float32),
            )

        @pl.when(first)
        def _():
            send(*pieces(own))

        @pl.when(jnp.logical_not(first))
        def _():
            part_copy(q, d, behind).wait_recv()
            summed = tuple(a + b for a, b in zip(pieces(own), pieces(pin)))

            @pl.when(last)
            def _():
                finish(l, q, d, *summed)
                hid_copy(q, d, behind).start()

            @pl.when(jnp.logical_not(last))
            def _():
                send(*summed)

    def spread_back(d, l, q):
        source = z + 1 if d == 0 else z - 1
        onward = z - 1 if d == 0 else z + 1
        last = (z == 0) if d == 0 else (z == R - 1)
        hid_copy(q, d, source).wait_recv()

        @pl.when(jnp.logical_not(last))
        def _():
            hid_copy(q, d, onward).start()

    def peer_copy(src, dst, send_sem, recv_sem, peer):
        return pltpu.make_async_remote_copy(
            src_ref=src,
            dst_ref=dst,
            send_sem=send_sem,
            recv_sem=recv_sem,
            device_id={"cb": peer},
            device_id_type=MESH,
        )

    def wait_group(ref, q, sem):
        view = ref.at[q, 0 : N - 1]
        pltpu.make_async_copy(view, view, sem).wait()

    def down_and_scatter(l, i, q):
        h = hid[q].reshape(rows, wide)
        product = jnp.dot(h, wd[l], preferred_element_type=jnp.float32)
        ro[q] = product.reshape(N, own_rows, Dl).astype(jnp.bfloat16)
        for k in range(1, N):
            peer = lax.rem(me + k, N)
            peer_copy(
                ro.at[q, peer], ri.at[q, me], rs_s.at[q], rs_r.at[q], peer
            ).start()
        ri[q, me] = ro[q, me]

    def sum_and_gather(l, i, q):
        wait_group(ri, q, rs_r.at[q])
        total = ri[q, 0].astype(jnp.float32)
        for k in range(1, N):
            total = total + ri[q, k].astype(jnp.float32)
        branch = total * ds_ref[pl.ds(l, 1), :]
        fresh = RESIDUAL_KEEP * xs[q, me].astype(jnp.float32) + branch
        xs[q + n, me] = fresh.astype(jnp.bfloat16)
        for k in range(1, N):
            peer = lax.rem(me + k, N)
            peer_copy(
                xs.at[q + n, me], xs.at[q + n, me], ag_s.at[q], ag_r.at[q], peer
            ).start()

    def gathered(l, i, q):
        wait_group(xs, q + n, ag_r.at[q])

        @pl.when(l == L - 1)
        def _():
            block = xs[q + n].astype(jnp.float32).reshape(rows, Dl)
            at = pl.ds(pl.multiple_of(i * rows, rows), rows)
            out_ref[at, :] = block.astype(jnp.bfloat16)

    def products(l, i, q):
        x = xs[q].astype(jnp.float32).reshape(rows, Dl)
        squares = jnp.sum(x * x, axis=1, keepdims=True)
        normed = (x * gain_ref[pl.ds(l, 1), :]).astype(jnp.bfloat16)
        result = lax.dot_general(
            normed,
            wc[l],
            (((1,), (1,)), ((), ())),
            preferred_element_type=jnp.float32,
        )
        tail_lane = lax.broadcasted_iota(jnp.int32, (rows, LANES), 1)
        tail = jnp.where(tail_lane == sq_lane, squares, result[:, 2 * full :])
        for d in range(2):
            part = slice(d * m, (d + 1) * m)
            own[q, d, :, 0 : 2 * full] = result[part, 0 : 2 * full]
            own[q, d, :, 2 * full :] = tail[part]

    def slot(t, carry):
        when_item(t - 1 - z, lambda l, i, q: chain(0, l, q))
        when_item(t - R + z, lambda l, i, q: chain(1, l, q))

        @pl.when(z < R - 1)
        def _():
            when_item(t - 2 * R + 1 + z, lambda l, i, q: spread_back(0, l, q))

        @pl.when(z > 0)
        def _():
            when_item(t - R - z, lambda l, i, q: spread_back(1, l, q))

        when_item(t - 2 * R + 1, down_and_scatter)
        for l in range(L):
            if l:
                pl.when(t == l * S - 4)(functools.partial(cast_up, l))
            pl.when(t == l * S + 1)(functools.partial(cast_down, l))

        when_item(t - 2 * R, gathered)
        when_item(t, products)
        when_item(t - 2 * R + 1, sum_and_gather)
        return carry

    lax.fori_loop(0, (L - 1) * S + n + 2 * R, slot, 0)

    def drain(q, carry):
        @pl.when(z < R - 1)
        def _():
            part_copy(q, 0, z + 1).wait_send()
            hid_copy(q, 1, z + 1).wait_send()

        @pl.when(z > 0)
        def _():
            part_copy(q, 1, z - 1).wait_send()
            hid_copy(q, 0, z - 1).wait_send()

        wait_group(ro, q, rs_s.at[q])
        wait_group(xs, q + n, ag_s.at[q])
        return carry

    lax.fori_loop(0, L * n, drain, 0)


def solution(mesh):
    R, N = mesh.shape["ra"], mesh.shape["cb"]

    def shards(*args):
        args = list(args)
        for k in (2, 4):
            args[k] = jnp.swapaxes(args[k], 1, 2)
        for k in (6, 7):
            args[k] = jnp.swapaxes(args[k], 0, 1)
        tokens, gw = args[0], args[2]
        T, Dl = tokens.shape
        L, F, _ = gw.shape
        m = 32
        rows = 2 * m
        n = T // rows
        full = F // LANES * LANES
        wide = full + LANES
        packed = 2 * full + LANES
        cfg = (R, N, L, n, m, Dl * R, F)
        Q = L * n
        bf16, f32 = jnp.bfloat16, jnp.float32
        dma = pltpu.SemaphoreType.DMA
        vmem = pl.BlockSpec(memory_space=pltpu.VMEM)
        hbm = pl.BlockSpec(memory_space=pl.ANY)
        in_specs = [hbm if k in (2, 4, 10) else vmem for k in range(12)]
        return pl.pallas_call(
            functools.partial(kernel, cfg),
            out_shape=jax.ShapeDtypeStruct((T, Dl), bf16),
            in_specs=in_specs,
            out_specs=vmem,
            scratch_shapes=[
                pltpu.VMEM((F, Dl), f32),
                pltpu.VMEM((F, Dl), f32),
                pltpu.VMEM((F, Dl), f32),
                pltpu.VMEM((L, packed, Dl), bf16),
                pltpu.VMEM((L, wide, Dl), bf16),
                pltpu.VMEM((L, 16, wide), f32),
                pltpu.VMEM((Q + n, N, rows // N, Dl), bf16),
                pltpu.VMEM((Q, 2, m, packed), f32),
                pltpu.VMEM((Q, 2, m, packed), bf16),
                pltpu.VMEM((Q, 2, m, packed), bf16),
                pltpu.VMEM((Q, 2, m, wide), bf16),
                pltpu.VMEM((Q, N, rows // N, Dl), bf16),
                pltpu.VMEM((Q, N, rows // N, Dl), bf16),
                dma((3,)),
                dma((Q, 2)),
                dma((Q, 2)),
                dma((Q, 2)),
                dma((Q, 2)),
                dma((Q,)),
                dma((Q,)),
                dma((Q,)),
                dma((Q,)),
            ],
            compiler_params=pltpu.CompilerParams(
                collective_id=0,
                has_side_effects=True,
                vmem_limit_bytes=67043328,
            ),
        )(*args)

    placed = (
        P(None, "ra"),
        P(None, "ra"),
        P(None, "ra", "cb"),
        P(None, "cb"),
        P(None, "ra", "cb"),
        P(None, "cb"),
        P(None, None, "cb"),
        P(None, None, "cb"),
        P(None, "cb"),
        P(None, "cb"),
        P(None, "cb", "ra"),
        P(None, "ra"),
    )
    return jax.shard_map(
        shards, mesh=mesh, in_specs=placed, out_specs=P(None, "ra"), check_vma=False
    )
```

profile of v0, /device:TPU:0, one launch (start us, length us, event | category | flops | bytes accessed | tf_op | source)
XLA Modules:
  0.0 129.2 jit_solution(10444062970384586826)
XLA Ops:
  0.0 127.2 %shard_map.118 = bf16[512,768]{1,0:T(8,128)(2,1)} custom-call(bf16[512,768]{1,0:T(8,128)(2,1)} %tokens_ref.1, f32[2,768]{1,0:T(2,128)} %gain_ref.1, f32[2,1056,768]{2,1,0:T(8,128)} %bitcast.4, f32[2,1056]{1,0:T(2,128)} %gs_ref.1, f32[2,1056,768]{2,1,0:T(8,128)} %bitcast.5, f32[2,1056]{1,0:T(2,128)} %vs_ref.1, f32[3,2,1056]{2,1,0:T(2,128)} %bitcast.6, ...), custom_call_target="tpu_custom_call" | custom-call | tf_op jit(solution)/shard_map/pallas_call | solution.py:379
  127.2 2.1 %copy.14 = bf16[512,768]{1,0:T(8,128)(2,1)} copy(bf16[512,768]{1,0:T(8,128)(2,1)} %shard_map.118) | data formatting | bytes 1572864
where the time goes:
time: 129 us
  Pallas kernels  127 us (98%)
  local copies, waits for them, and re-layouts  2.06 us (2%)
    pallas_call x1, Pallas kernels, shards(): pl.pallas_call(functools.partial(kernel, cfg), out_shape=jax.ShapeDtypeSt...  127 us

commit v1 on v0

--- a/solution.py
+++ b/solution.py
@@ -11,6 +11,11 @@
 RESIDUAL_KEEP = 0.5
 MESH = pl.DeviceIdType.MESH
 LANES = 128
+FIRST = 1
+HOP = 2
+BACK = 2
+SUM_GAP = 2
+GATHER_GAP = 2
 
 
 def kernel(
@@ -54,13 +59,19 @@
     R, N, L, n, m, D, F = cfg
     Dl = tokens_ref.shape[1]
     rows = 2 * m
-    own_rows = rows // N
+    RG = rows // SEQ_LEN
+    CG = N // RG
+    Dc = Dl // CG
     taps = gc_ref.shape[0]
     full = F // LANES * LANES
     rest = F - full
     wide = full + LANES
     sq_lane = 2 * rest
-    S = max(n, 2 * R)
+    at_last = FIRST + (R - 1) * HOP
+    at_down = at_last + (R - 1) * BACK
+    at_sum = at_down + SUM_GAP
+    at_gather = at_sum + GATHER_GAP
+    S = max(n, at_gather)
     z = lax.axis_index("ra")
     me = lax.axis_index("cb")
 
@@ -85,9 +96,26 @@
     def _():
         pl.semaphore_signal(barrier, inc=1, device_id={"ra": z + 1}, device_id_type=MESH)
 
-    for i in range(n):
-        block = tokens_ref[i * rows : (i + 1) * rows, :].astype(jnp.float32)
-        xs[i] = block.reshape(N, own_rows, Dl).astype(jnp.bfloat16)
+    def split(block):
+        return [
+            block[:, c * Dc : (c + 1) * Dc].reshape(RG, SEQ_LEN, Dc).astype(jnp.bfloat16)
+            for c in range(CG)
+        ]
+
+    def joined(q):
+        parts = [
+            xs[q, c * RG : (c + 1) * RG].astype(jnp.float32).reshape(rows, Dc)
+            for c in range(CG)
+        ]
+        return jnp.concatenate(parts, axis=1) if CG > 1 else parts[0]
+
+    def take(i, carry):
+        at = pl.ds(pl.multiple_of(i * rows, rows), rows)
+        for c, piece in enumerate(split(tokens_ref[at, :].astype(jnp.float32))):
+            xs[i, c * RG : (c + 1) * RG] = piece
+        return carry
+
+    lax.fori_loop(0, n, take, 0)
 
     par[...] = jnp.zeros_like(par)
     for l in range(L):
@@ -108,24 +136,59 @@
 
         lax.fori_loop(0, count // step, move, 0)
 
+    def fetch(l, k):
+        if l < L:
+            weight_copy(l, k).start()
+
     def cast_up(l):
         weight_copy(l, 0).wait()
         cast_rows(wc, l, 0, stage_g, 0, full, 64)
         cast_rows(wc, l, 2 * full, stage_g, full, rest, 32)
+        fetch(l + 1, 0)
         weight_copy(l, 1).wait()
         cast_rows(wc, l, full, stage_v, 0, full, 64)
         cast_rows(wc, l, 2 * full + rest, stage_v, full, rest, 32)
         wc[l, 2 * F :, :] = jnp.zeros((wc.shape[1] - 2 * F, Dl), jnp.bfloat16)
-        if l + 1 < L:
-            weight_copy(l + 1, 0).start()
-            weight_copy(l + 1, 1).start()
+        fetch(l + 1, 1)
 
     def cast_down(l):
         weight_copy(l, 2).wait()
         cast_rows(wd, l, 0, stage_d, 0, F, 32)
         wd[l, F:wide, :] = jnp.zeros((wide - F, Dl), jnp.bfloat16)
-        if l + 1 < L:
-            weight_copy(l + 1, 2).start()
+        fetch(l + 1, 2)
+
+    pieces_up = full // 64
+    lag = pieces_up // 4
+    pieces_down = -(-(F // 32) // (pieces_up - lag))
+
+    def cast_piece(l, c):
+        @pl.when(c == 0)
+        def _():
+            weight_copy(l, 0).wait()
+            weight_copy(l, 1).wait()
+            cast_rows(wc, l, 2 * full, stage_g, full, rest, 32)
+            cast_rows(wc, l, 2 * full + rest, stage_v, full, rest, 32)
+            wc[l, 2 * F :, :] = jnp.zeros((wc.shape[1] - 2 * F, Dl), jnp.bfloat16)
+
+        @pl.when(c == lag)
+        def _():
+            weight_copy(l, 2).wait()
+            wd[l, F:wide, :] = jnp.zeros((wide - F, Dl), jnp.bfloat16)
+
+        cast_rows(wc, l, c * 64, stage_g, c * 64, 64, 64)
+        cast_rows(wc, l, full + c * 64, stage_v, c * 64, 64, 64)
+        for k in range(pieces_down):
+
+            b = (c - lag) * pieces_down + k
+
+            @pl.when((b >= 0) & (b < F // 32))
+            def _():
+                cast_rows(wd, l, b * 32, stage_d, b * 32, 32, 32)
+
+        @pl.when(c == pieces_up - 1)
+        def _():
+            for k in range(3):
+                fetch(l + 1, k)
 
     cast_up(0)
 
@@ -260,7 +323,8 @@
     def down_and_scatter(l, i, q):
         h = hid[q].reshape(rows, wide)
         product = jnp.dot(h, wd[l], preferred_element_type=jnp.float32)
-        ro[q] = product.reshape(N, own_rows, Dl).astype(jnp.bfloat16)
+        for c, piece in enumerate(split(product)):
+            ro[q, c * RG : (c + 1) * RG] = piece
         for k in range(1, N):
             peer = lax.rem(me + k, N)
             peer_copy(
@@ -273,7 +337,12 @@
         total = ri[q, 0].astype(jnp.float32)
         for k in range(1, N):
             total = total + ri[q, k].astype(jnp.float32)
-        branch = total * ds_ref[pl.ds(l, 1), :]
+        scales = ds_ref[pl.ds(l, 1), :]
+        mine = lax.div(me, RG)
+        scale = scales[:, 0:Dc]
+        for c in range(1, CG):
+            scale = jnp.where(mine == c, scales[:, c * Dc : (c + 1) * Dc], scale)
+        branch = total * scale
         fresh = RESIDUAL_KEEP * xs[q, me].astype(jnp.float32) + branch
         xs[q + n, me] = fresh.astype(jnp.bfloat16)
         for k in range(1, N):
@@ -287,12 +356,12 @@
 
         @pl.when(l == L - 1)
         def _():
-            block = xs[q + n].astype(jnp.float32).reshape(rows, Dl)
+            block = joined(q + n)
             at = pl.ds(pl.multiple_of(i * rows, rows), rows)
             out_ref[at, :] = block.astype(jnp.bfloat16)
 
     def products(l, i, q):
-        x = xs[q].astype(jnp.float32).reshape(rows, Dl)
+        x = joined(q)
         squares = jnp.sum(x * x, axis=1, keepdims=True)
         normed = (x * gain_ref[pl.ds(l, 1), :]).astype(jnp.bfloat16)
         result = lax.dot_general(
@@ -309,29 +378,33 @@
             own[q, d, :, 2 * full :] = tail[part]
 
     def slot(t, carry):
-        when_item(t - 1 - z, lambda l, i, q: chain(0, l, q))
-        when_item(t - R + z, lambda l, i, q: chain(1, l, q))
+        when_item(t - FIRST - HOP * z, lambda l, i, q: chain(0, l, q))
+        when_item(t - FIRST - HOP * (R - 1 - z), lambda l, i, q: chain(1, l, q))
 
         @pl.when(z < R - 1)
         def _():
-            when_item(t - 2 * R + 1 + z, lambda l, i, q: spread_back(0, l, q))
+            ago = at_last + BACK * (R - 1 - z)
+            when_item(t - ago, lambda l, i, q: spread_back(0, l, q))
 
         @pl.when(z > 0)
         def _():
-            when_item(t - R - z, lambda l, i, q: spread_back(1, l, q))
-
-        when_item(t - 2 * R + 1, down_and_scatter)
-        for l in range(L):
-            if l:
-                pl.when(t == l * S - 4)(functools.partial(cast_up, l))
-            pl.when(t == l * S + 1)(functools.partial(cast_down, l))
-
-        when_item(t - 2 * R, gathered)
+            when_item(t - at_last - BACK * z, lambda l, i, q: spread_back(1, l, q))
+
+        when_item(t - at_down, down_and_scatter)
+        when_item(t - at_sum, sum_and_gather)
+        when_item(t - at_gather, gathered)
         when_item(t, products)
-        when_item(t - 2 * R + 1, sum_and_gather)
+        pl.when(t == 1)(functools.partial(cast_down, 0))
+        for l in range(1, L):
+            c = t - l * S + pieces_up
+
+            @pl.when((c >= 0) & (c < pieces_up))
+            def _():
+                cast_piece(l, c)
+
         return carry
 
-    lax.fori_loop(0, (L - 1) * S + n + 2 * R, slot, 0)
+    lax.fori_loop(0, (L - 1) * S + n + at_gather, slot, 0)
 
     def drain(q, carry):
         @pl.when(z < R - 1)
@@ -363,8 +436,11 @@
         tokens, gw = args[0], args[2]
         T, Dl = tokens.shape
         L, F, _ = gw.shape
-        m = 32
+        m = 16
+        if N * SEQ_LEN > 2 * m and Dl % (N * SEQ_LEN // (2 * m) * LANES):
+            m = N * SEQ_LEN // 2
         rows = 2 * m
+        parts = N * SEQ_LEN // rows
         n = T // rows
         full = F // LANES * LANES
         wide = full + LANES
@@ -388,13 +464,13 @@
                 pltpu.VMEM((L, packed, Dl), bf16),
                 pltpu.VMEM((L, wide, Dl), bf16),
                 pltpu.VMEM((L, 16, wide), f32),
-                pltpu.VMEM((Q + n, N, rows // N, Dl), bf16),
+                pltpu.VMEM((Q + n, N, SEQ_LEN, Dl // parts), bf16),
                 pltpu.VMEM((Q, 2, m, packed), f32),
                 pltpu.VMEM((Q, 2, m, packed), bf16),
                 pltpu.VMEM((Q, 2, m, packed), bf16),
                 pltpu.VMEM((Q, 2, m, wide), bf16),
-                pltpu.VMEM((Q, N, rows // N, Dl), bf16),
-                pltpu.VMEM((Q, N, rows // N, Dl), bf16),
+                pltpu.VMEM((Q, N, SEQ_LEN, Dl // parts), bf16),
+                pltpu.VMEM((Q, N, SEQ_LEN, Dl // parts), bf16),
                 dma((3,)),
                 dma((Q, 2)),
                 dma((Q, 2)),

time: 129 us -> 114 us (0.88)
  Pallas kernels: 127 us -> 112 us
    pallas_call x1, Pallas kernels: 127 us -> 112 us  [shards(): pl.pallas_call(functools.partial(kernel, cfg), out_shape=jax.ShapeDtypeSt...]
where the time goes in v1:
time: 114 us
  Pallas kernels  112 us (98%)
  local copies, waits for them, and re-layouts  2.06 us (2%)
    pallas_call x1, Pallas kernels, shards(): pl.pallas_call(functools.partial(kernel, cfg), out_shape=jax.ShapeDtypeSt...  112 us

profile of v1, /device:TPU:0, one launch (start us, length us, event | category | flops | bytes accessed | tf_op | source)
XLA Modules:
  0.0 113.6 jit_solution(1256491791459371946)
XLA Ops:
  0.0 111.6 %shard_map.118 = bf16[512,768]{1,0:T(8,128)(2,1)} custom-call(bf16[512,768]{1,0:T(8,128)(2,1)} %tokens_ref.1, f32[2,768]{1,0:T(2,128)} %gain_ref.1, f32[2,1056,768]{2,1,0:T(8,128)} %bitcast.4, f32[2,1056]{1,0:T(2,128)} %gs_ref.1, f32[2,1056,768]{2,1,0:T(8,128)} %bitcast.5, f32[2,1056]{1,0:T(2,128)} %vs_ref.1, f32[3,2,1056]{2,1,0:T(2,128)} %bitcast.6, ...), custom_call_target="tpu_custom_call" | custom-call | tf_op jit(solution)/shard_map/pallas_call | solution.py:455
  111.6 2.1 %copy.14 = bf16[512,768]{1,0:T(8,128)(2,1)} copy(bf16[512,768]{1,0:T(8,128)(2,1)} %shard_map.118) | data formatting | bytes 1572864

commit v2 on v1

--- a/solution.py
+++ b/solution.py
@@ -16,23 +16,34 @@
 BACK = 2
 SUM_GAP = 2
 GATHER_GAP = 2
+DIRECT = 2
+DIRECT_GAP = 3
 
 
 def kernel(
     cfg,
+    tokens_in,
+    gain_in,
+    gw_ref,
+    gs_in,
+    vw_ref,
+    vs_in,
+    gc_in,
+    vc_in,
+    gb_in,
+    vb_in,
+    dw_ref,
+    ds_in,
+    out_ref,
     tokens_ref,
     gain_ref,
-    gw_ref,
     gs_ref,
-    vw_ref,
     vs_ref,
     gc_ref,
     vc_ref,
     gb_ref,
     vb_ref,
-    dw_ref,
     ds_ref,
-    out_ref,
     stage_g,
     stage_v,
     stage_d,
@@ -47,9 +58,12 @@
     ro,
     ri,
     w_sem,
+    first_sem,
+    in_sem,
     ps,
     pr,
     hs,
+    hs_far,
     hr,
     rs_s,
     rs_r,
@@ -72,6 +86,11 @@
     at_sum = at_down + SUM_GAP
     at_gather = at_sum + GATHER_GAP
     S = max(n, at_gather)
+    K = hs_far.shape[0]
+    far_down = at_last + DIRECT_GAP
+    far_sum = far_down + SUM_GAP
+    far_gather = far_sum + GATHER_GAP
+    outer = L * n - K
     z = lax.axis_index("ra")
     me = lax.axis_index("cb")
 
@@ -79,8 +98,21 @@
         src, dst = ((gw_ref, stage_g), (vw_ref, stage_v), (dw_ref, stage_d))[k]
         return pltpu.make_async_copy(src.at[l], dst, w_sem.at[k])
 
-    for k in range(3):
-        weight_copy(0, k).start()
+    small = (
+        (tokens_in, tokens_ref),
+        (gain_in, gain_ref),
+        (gs_in, gs_ref),
+        (vs_in, vs_ref),
+        (gc_in, gc_ref),
+        (vc_in, vc_ref),
+        (gb_in, gb_ref),
+        (vb_in, vb_ref),
+        (ds_in, ds_ref),
+    )
+    inputs = [
+        pltpu.make_async_copy(src, dst, in_sem.at[k])
+        for k, (src, dst) in enumerate(small)
+    ]
 
     barrier = pltpu.get_barrier_semaphore()
     for k in range(1, N):
@@ -95,6 +127,25 @@
     @pl.when(z < R - 1)
     def _():
         pl.semaphore_signal(barrier, inc=1, device_id={"ra": z + 1}, device_id_type=MESH)
+
+    C = first_sem.shape[1]
+    step = full // C
+
+    def first_copy(k, c):
+        src, dst = ((gw_ref, stage_g), (vw_ref, stage_v))[k]
+        at = pl.ds(c * step, step + (rest if c == C - 1 else 0))
+        return pltpu.make_async_copy(
+            src.at[0, at, :], dst.at[at, :], first_sem.at[k, c]
+        )
+
+    inputs[0].start()
+    inputs[1].start()
+    for c in range(C):
+        first_copy(0, c).start()
+        first_copy(1, c).start()
+    for k in range(2, len(inputs)):
+        inputs[k].start()
+    weight_copy(0, 2).start()
 
     def split(block):
         return [
@@ -109,23 +160,26 @@
         ]
         return jnp.concatenate(parts, axis=1) if CG > 1 else parts[0]
 
-    def take(i, carry):
+    def take(i):
         at = pl.ds(pl.multiple_of(i * rows, rows), rows)
         for c, piece in enumerate(split(tokens_ref[at, :].astype(jnp.float32))):
             xs[i, c * RG : (c + 1) * RG] = piece
-        return carry
-
-    lax.fori_loop(0, n, take, 0)
-
-    par[...] = jnp.zeros_like(par)
-    for l in range(L):
-        par[l, 0:1, 0:F] = gs_ref[l : l + 1, :]
-        par[l, 1:2, 0:F] = vs_ref[l : l + 1, :]
-        par[l, 2:3, 0:F] = gb_ref[l : l + 1, :]
-        par[l, 3:4, 0:F] = vb_ref[l : l + 1, :]
-        for k in range(taps):
-            par[l, 4 + k : 5 + k, 0:F] = gc_ref[k, l : l + 1, :]
-            par[l, 4 + taps + k : 5 + taps + k, 0:F] = vc_ref[k, l : l + 1, :]
+
+    inputs[0].wait()
+    take(0)
+
+    def set_par():
+        for k in range(2, len(inputs)):
+            inputs[k].wait()
+        par[...] = jnp.zeros_like(par)
+        for l in range(L):
+            par[l, 0:1, 0:F] = gs_ref[l : l + 1, :]
+            par[l, 1:2, 0:F] = vs_ref[l : l + 1, :]
+            par[l, 2:3, 0:F] = gb_ref[l : l + 1, :]
+            par[l, 3:4, 0:F] = vb_ref[l : l + 1, :]
+            for k in range(taps):
+                par[l, 4 + k : 5 + k, 0:F] = gc_ref[k, l : l + 1, :]
+                par[l, 4 + taps + k : 5 + taps + k, 0:F] = vc_ref[k, l : l + 1, :]
 
     def cast_rows(dst, l, first, src, start, count, step):
         def move(b, carry):
@@ -140,68 +194,96 @@
         if l < L:
             weight_copy(l, k).start()
 
-    def cast_up(l):
-        weight_copy(l, 0).wait()
-        cast_rows(wc, l, 0, stage_g, 0, full, 64)
+    def cast_rest(l):
         cast_rows(wc, l, 2 * full, stage_g, full, rest, 32)
-        fetch(l + 1, 0)
-        weight_copy(l, 1).wait()
-        cast_rows(wc, l, full, stage_v, 0, full, 64)
         cast_rows(wc, l, 2 * full + rest, stage_v, full, rest, 32)
         wc[l, 2 * F :, :] = jnp.zeros((wc.shape[1] - 2 * F, Dl), jnp.bfloat16)
-        fetch(l + 1, 1)
-
-    def cast_down(l):
-        weight_copy(l, 2).wait()
-        cast_rows(wd, l, 0, stage_d, 0, F, 32)
-        wd[l, F:wide, :] = jnp.zeros((wide - F, Dl), jnp.bfloat16)
-        fetch(l + 1, 2)
-
-    pieces_up = full // 64
-    lag = pieces_up // 4
-    pieces_down = -(-(F // 32) // (pieces_up - lag))
-
-    def cast_piece(l, c):
+
+    up_rows = full // 8
+    down_rows = 96
+
+    def cast_up_piece(l, c):
         @pl.when(c == 0)
         def _():
             weight_copy(l, 0).wait()
             weight_copy(l, 1).wait()
-            cast_rows(wc, l, 2 * full, stage_g, full, rest, 32)
-            cast_rows(wc, l, 2 * full + rest, stage_v, full, rest, 32)
-            wc[l, 2 * F :, :] = jnp.zeros((wc.shape[1] - 2 * F, Dl), jnp.bfloat16)
-
-        @pl.when(c == lag)
+            cast_rest(l)
+
+        cast_rows(wc, l, c * up_rows, stage_g, c * up_rows, up_rows, 64)
+        cast_rows(wc, l, full + c * up_rows, stage_v, c * up_rows, up_rows, 64)
+
+        @pl.when(c == 7)
+        def _():
+            fetch(l + 1, 0)
+            fetch(l + 1, 1)
+
+    def cast_down_piece(l, c):
+        @pl.when(c == 0)
         def _():
             weight_copy(l, 2).wait()
             wd[l, F:wide, :] = jnp.zeros((wide - F, Dl), jnp.bfloat16)
 
-        cast_rows(wc, l, c * 64, stage_g, c * 64, 64, 64)
-        cast_rows(wc, l, full + c * 64, stage_v, c * 64, 64, 64)
-        for k in range(pieces_down):
-
-            b = (c - lag) * pieces_down + k
-
-            @pl.when((b >= 0) & (b < F // 32))
-            def _():
-                cast_rows(wd, l, b * 32, stage_d, b * 32, 32, 32)
-
-        @pl.when(c == pieces_up - 1)
-        def _():
-            for k in range(3):
-                fetch(l + 1, k)
-
-    cast_up(0)
-
+        cast_rows(wd, l, c * down_rows, stage_d, c * down_rows, down_rows, 32)
+
+        @pl.when(c == F // down_rows - 1)
+        def _():
+            fetch(l + 1, 2)
+
+    def normalised(l, q):
+        x = joined(q)
+        squares = jnp.sum(x * x, axis=1, keepdims=True)
+        return squares, (x * gain_ref[pl.ds(l, 1), :]).astype(jnp.bfloat16)
+
+    def times_up(normed, l, lo, hi):
+        return lax.dot_general(
+            normed,
+            wc[l, lo:hi, :],
+            (((1,), (1,)), ((), ())),
+            preferred_element_type=jnp.float32,
+        )
+
+    def keep(q, lo, hi, result):
+        for d in range(2):
+            own[q, d, :, lo:hi] = result[d * m : (d + 1) * m]
+
+    def keep_tail(q, result, squares):
+        at = lax.broadcasted_iota(jnp.int32, (rows, LANES), 1)
+        keep(q, 2 * full, 2 * full + LANES, jnp.where(at == sq_lane, squares, result))
+
+    inputs[1].wait()
+    squares, normed = normalised(0, 0)
+    for c in range(C):
+        first_copy(0, c).wait()
+        cast_rows(wc, 0, c * step, stage_g, c * step, step, 64)
+        keep(0, c * step, (c + 1) * step, times_up(normed, 0, c * step, (c + 1) * step))
+        first_copy(1, c).wait()
+        lo = full + c * step
+        cast_rows(wc, 0, lo, stage_v, c * step, step, 64)
+        keep(0, lo, lo + step, times_up(normed, 0, lo, lo + step))
+    cast_rest(0)
+    keep_tail(0, times_up(normed, 0, 2 * full, 2 * full + LANES), squares)
+
+    set_par()
+    for k in range(2):
+        fetch(1, k)
     expected = N - 1 + jnp.where(z > 0, 1, 0) + jnp.where(z < R - 1, 1, 0)
     pl.semaphore_wait(barrier, expected)
 
-    def when_item(g, fn):
+    def when_item(g, fn, end=L * n):
         layer = lax.div(g, S)
         i = lax.rem(g, S)
-
-        @pl.when((g >= 0) & (g < L * S) & (i < n))
-        def _():
-            fn(layer, i, layer * n + i)
+        q = layer * n + i
+
+        @pl.when((g >= 0) & (g < L * S) & (i < n) & (q < end))
+        def _():
+            fn(layer, i, q)
+
+    def when_far(g, fn):
+        i = g - (L - 1) * S
+
+        @pl.when((i >= n - K) & (i < n))
+        def _():
+            fn(L - 1, i, (L - 1) * n + i)
 
     def part_copy(q, d, target):
         return pltpu.make_async_remote_copy(
@@ -220,6 +302,16 @@
             send_sem=hs.at[q, d],
             recv_sem=hr.at[q, d],
             device_id={"ra": target},
+            device_id_type=MESH,
+        )
+
+    def far_copy(q, d, k):
+        return pltpu.make_async_remote_copy(
+            src_ref=hid.at[q, d],
+            dst_ref=hid.at[q, d],
+            send_sem=hs_far.at[q - outer, d, k],
+            recv_sem=hr.at[q, d],
+            device_id={"ra": k if d == 0 else R - 1 - k},
             device_id_type=MESH,
         )
 
@@ -290,7 +382,15 @@
             @pl.when(last)
             def _():
                 finish(l, q, d, *summed)
-                hid_copy(q, d, behind).start()
+
+                @pl.when(q < outer)
+                def _():
+                    hid_copy(q, d, behind).start()
+
+                @pl.when(q >= outer)
+                def _():
+                    for k in range(R - 1):
+                        far_copy(q, d, k).start()
 
             @pl.when(jnp.logical_not(last))
             def _():
@@ -361,61 +461,86 @@
             out_ref[at, :] = block.astype(jnp.bfloat16)
 
     def products(l, i, q):
-        x = joined(q)
-        squares = jnp.sum(x * x, axis=1, keepdims=True)
-        normed = (x * gain_ref[pl.ds(l, 1), :]).astype(jnp.bfloat16)
-        result = lax.dot_general(
-            normed,
-            wc[l],
-            (((1,), (1,)), ((), ())),
-            preferred_element_type=jnp.float32,
-        )
-        tail_lane = lax.broadcasted_iota(jnp.int32, (rows, LANES), 1)
-        tail = jnp.where(tail_lane == sq_lane, squares, result[:, 2 * full :])
-        for d in range(2):
-            part = slice(d * m, (d + 1) * m)
-            own[q, d, :, 0 : 2 * full] = result[part, 0 : 2 * full]
-            own[q, d, :, 2 * full :] = tail[part]
+        squares, normed = normalised(l, q)
+        result = times_up(normed, l, 0, 2 * full + LANES)
+        keep(q, 0, 2 * full, result[:, 0 : 2 * full])
+        keep_tail(q, result[:, 2 * full :], squares)
+
+    def far_down_and_scatter(l, i, q):
+        @pl.when(z < R - 1)
+        def _():
+            hid_copy(q, 0, z).wait_recv()
+
+        @pl.when(z > 0)
+        def _():
+            hid_copy(q, 1, z).wait_recv()
+
+        down_and_scatter(l, i, q)
 
     def slot(t, carry):
+
+        @pl.when(z < R - 1)
+        def _():
+            ago = at_last + BACK * (R - 1 - z)
+            when_item(t - ago, lambda l, i, q: spread_back(0, l, q), outer)
+
+        @pl.when(z > 0)
+        def _():
+            ago = at_last + BACK * z
+            when_item(t - ago, lambda l, i, q: spread_back(1, l, q), outer)
+
+        when_item(t - at_down, down_and_scatter, outer)
+        when_far(t - far_down, far_down_and_scatter)
+        when_item(t - at_sum, sum_and_gather, outer)
+        when_far(t - far_sum, sum_and_gather)
         when_item(t - FIRST - HOP * z, lambda l, i, q: chain(0, l, q))
         when_item(t - FIRST - HOP * (R - 1 - z), lambda l, i, q: chain(1, l, q))
-
-        @pl.when(z < R - 1)
-        def _():
-            ago = at_last + BACK * (R - 1 - z)
-            when_item(t - ago, lambda l, i, q: spread_back(0, l, q))
-
-        @pl.when(z > 0)
-        def _():
-            when_item(t - at_last - BACK * z, lambda l, i, q: spread_back(1, l, q))
-
-        when_item(t - at_down, down_and_scatter)
-        when_item(t - at_sum, sum_and_gather)
-        when_item(t - at_gather, gathered)
+        when_item(t - at_gather, gathered, outer)
+        when_far(t - far_gather, gathered)
+        pl.when(t < n)(lambda: take(t))
         when_item(t, products)
-        pl.when(t == 1)(functools.partial(cast_down, 0))
+
+        pl.when((t >= 2) & (t < 2 + F // down_rows))(
+            functools.partial(cast_down_piece, 0, t - 2)
+        )
         for l in range(1, L):
-            c = t - l * S + pieces_up
-
-            @pl.when((c >= 0) & (c < pieces_up))
-            def _():
-                cast_piece(l, c)
+            c = t - (l - 1) * S - 4
+            pl.when((c >= 0) & (c < 8))(functools.partial(cast_up_piece, l, c))
+            pl.when((c >= 10) & (c < 10 + F // down_rows))(
+                functools.partial(cast_down_piece, l, c - 10)
+            )
 
         return carry
 
-    lax.fori_loop(0, (L - 1) * S + n + at_gather, slot, 0)
+    slots = max(n - K + at_gather, n + far_gather)
+    lax.fori_loop(1, (L - 1) * S + slots, slot, 0)
 
     def drain(q, carry):
         @pl.when(z < R - 1)
         def _():
             part_copy(q, 0, z + 1).wait_send()
+
+        @pl.when(z > 0)
+        def _():
+            part_copy(q, 1, z - 1).wait_send()
+
+        @pl.when((z < R - 1) & (q < outer))
+        def _():
             hid_copy(q, 1, z + 1).wait_send()
 
-        @pl.when(z > 0)
-        def _():
-            part_copy(q, 1, z - 1).wait_send()
+        @pl.when((z > 0) & (q < outer))
+        def _():
             hid_copy(q, 0, z - 1).wait_send()
+
+        for k in range(R - 1):
+
+            @pl.when((z == R - 1) & (q >= outer))
+            def _():
+                far_copy(q, 0, k).wait_send()
+
+            @pl.when((z == 0) & (q >= outer))
+            def _():
+                far_copy(q, 1, k).wait_send()
 
         wait_group(ro, q, rs_s.at[q])
         wait_group(xs, q + n, ag_s.at[q])
@@ -449,15 +574,20 @@
         Q = L * n
         bf16, f32 = jnp.bfloat16, jnp.float32
         dma = pltpu.SemaphoreType.DMA
-        vmem = pl.BlockSpec(memory_space=pltpu.VMEM)
         hbm = pl.BlockSpec(memory_space=pl.ANY)
-        in_specs = [hbm if k in (2, 4, 10) else vmem for k in range(12)]
-        return pl.pallas_call(
+        in_specs = [hbm] * len(args)
+        staged = [
+            pltpu.VMEM(a.shape, a.dtype)
+            for k, a in enumerate(args)
+            if k not in (2, 4, 10)
+        ]
+        held = pl.pallas_call(
             functools.partial(kernel, cfg),
-            out_shape=jax.ShapeDtypeStruct((T, Dl), bf16),
+            out_shape=pltpu.VMEM((T, Dl), bf16),
             in_specs=in_specs,
-            out_specs=vmem,
-            scratch_shapes=[
+            out_specs=pl.BlockSpec(memory_space=pltpu.VMEM),
+            scratch_shapes=staged
+            + [
                 pltpu.VMEM((F, Dl), f32),
                 pltpu.VMEM((F, Dl), f32),
                 pltpu.VMEM((F, Dl), f32),
@@ -472,9 +602,12 @@
                 pltpu.VMEM((Q, N, SEQ_LEN, Dl // parts), bf16),
                 pltpu.VMEM((Q, N, SEQ_LEN, Dl // parts), bf16),
                 dma((3,)),
+                dma((2, 4)),
+                dma((len(staged),)),
                 dma((Q, 2)),
                 dma((Q, 2)),
                 dma((Q, 2)),
+                dma((min(DIRECT, n), 2, R - 1)),
                 dma((Q, 2)),
                 dma((Q,)),
                 dma((Q,)),
@@ -484,9 +617,10 @@
             compiler_params=pltpu.CompilerParams(
                 collective_id=0,
                 has_side_effects=True,
-                vmem_limit_bytes=67043328,
+                vmem_limit_bytes=60 * 2**20,
             ),
         )(*args)
+        return held
 
     placed = (
         P(None, "ra"),

time: 114 us -> 108 us (0.947)
  Pallas kernels: 112 us -> 107 us
  local copies, waits for them, and re-layouts: 2.06 us -> 0.88 us
    pallas_call x1, Pallas kernels: 112 us -> 107 us  [shards(): pl.pallas_call(functools.partial(kernel, cfg), out_shape=pltpu.VMEM((T, D...]
    unnamed x1, local copies, waits for them, and re-layouts: 2.06 us -> 0.88 us
where the time goes in v2:
time: 108 us
  Pallas kernels  107 us (99%)
    pallas_call x1, Pallas kernels, shards(): pl.pallas_call(functools.partial(kernel, cfg), out_shape=pltpu.VMEM((T, D...  107 us

profile of v2, /device:TPU:0, one launch (start us, length us, event | category | flops | bytes accessed | tf_op | source)
XLA Modules:
  0.0 108.2 jit_solution(14117347515597060250)
XLA Ops:
  0.0 107.3 %shard_map.118 = bf16[512,768]{1,0:T(8,128)(2,1)S(1)} custom-call(bf16[512,768]{1,0:T(8,128)(2,1)} %tokens_in.1, f32[2,768]{1,0:T(2,128)} %gain_in.1, f32[2,1056,768]{2,1,0:T(8,128)} %bitcast.4, f32[2,1056]{1,0:T(2,128)} %gs_in.1, f32[2,1056,768]{2,1,0:T(8,128)} %bitcast.5, f32[2,1056]{1,0:T(2,128)} %vs_in.1, f32[3,2,1056]{2,1,0:T(2,128)} %bitcast.6, ...), custom_call_target="tpu_custom_call" | custom-call | tf_op jit(solution)/shard_map/pallas_call | solution.py:584
  107.4 0.9 copy.14

commit v3 on v2

--- a/solution.py
+++ b/solution.py
@@ -16,7 +16,7 @@
 BACK = 2
 SUM_GAP = 2
 GATHER_GAP = 2
-DIRECT = 2
+DIRECT = 3
 DIRECT_GAP = 3
 
 
@@ -317,6 +317,9 @@
 
     row_in_seq = lax.rem(lax.broadcasted_iota(jnp.int32, (m, wide), 0), SEQ_LEN)
     lane = lax.broadcasted_iota(jnp.int32, (m, LANES), 1)
+    tail_lane = lax.broadcasted_iota(jnp.int32, (SEQ_LEN, LANES), 1)
+    G = m // SEQ_LEN
+    tiles = full // LANES
 
     def conv(values, l, first):
         total = values * par[l, first + taps - 1 : first + taps, :]
@@ -338,7 +341,16 @@
         value = value * inverse * par[l, 1:2, :]
         gate = par[l, 2:3, :] + conv(gate, l, 4)
         value = par[l, 3:4, :] + conv(value, l, 4 + taps)
-        hid[q, d] = (gate / (1.0 + jnp.exp(-gate)) * value).astype(jnp.bfloat16)
+        hidden = gate / (1.0 + jnp.exp(-gate)) * value
+        packed = jnp.zeros((SEQ_LEN, LANES), jnp.float32)
+        for g in range(G):
+            piece = hidden[g * SEQ_LEN : (g + 1) * SEQ_LEN, :]
+            for c in range(tiles):
+                part = piece[:, c * LANES : (c + 1) * LANES]
+                hid[q, d, g * tiles + c] = part.astype(jnp.bfloat16)
+            piece = jnp.where(tail_lane < rest, piece[:, full:wide], 0.0)
+            packed = packed + (pltpu.roll(piece, g * rest, 1) if g else piece)
+        hid[q, d, G * tiles] = packed.astype(jnp.bfloat16)
 
     def chain(d, l, q):
         first = (z == 0) if d == 0 else (z == R - 1)
@@ -421,7 +433,15 @@
         pltpu.make_async_copy(view, view, sem).wait()
 
     def down_and_scatter(l, i, q):
-        h = hid[q].reshape(rows, wide)
+        lines = []
+        for d in range(2):
+            packed = hid[q, d, G * tiles].astype(jnp.float32)
+            for g in range(G):
+                line = [hid[q, d, g * tiles + c].astype(jnp.float32) for c in range(tiles)]
+                piece = pltpu.roll(packed, LANES - g * rest, 1) if g else packed
+                line.append(jnp.where(tail_lane < rest, piece, 0.0))
+                lines.append(jnp.concatenate(line, axis=1))
+        h = jnp.concatenate(lines, axis=0).astype(jnp.bfloat16)
         product = jnp.dot(h, wd[l], preferred_element_type=jnp.float32)
         for c, piece in enumerate(split(product)):
             ro[q, c * RG : (c + 1) * RG] = piece
@@ -598,7 +618,7 @@
                 pltpu.VMEM((Q, 2, m, packed), f32),
                 pltpu.VMEM((Q, 2, m, packed), bf16),
                 pltpu.VMEM((Q, 2, m, packed), bf16),
-                pltpu.VMEM((Q, 2, m, wide), bf16),
+                pltpu.VMEM((Q, 2, m // SEQ_LEN * (full // LANES) + 1, SEQ_LEN, LANES), bf16),
                 pltpu.VMEM((Q, N, SEQ_LEN, Dl // parts), bf16),
                 pltpu.VMEM((Q, N, SEQ_LEN, Dl // parts), bf16),
                 dma((3,)),

time: 108 us -> 107 us (level)
    pallas_call x1, Pallas kernels: 107 us -> 106 us  [shards(): pl.pallas_call(functools.partial(kernel, cfg), out_shape=pltpu.VMEM((T, D...]
where the time goes in v3:
time: 107 us
  Pallas kernels  106 us (99%)
    pallas_call x1, Pallas kernels, shards(): pl.pallas_call(functools.partial(kernel, cfg), out_shape=pltpu.VMEM((T, D...  106 us

profile of v3, /device:TPU:0, one launch (start us, length us, event | category | flops | bytes accessed | tf_op | source)
XLA Modules:
  0.0 106.8 jit_solution(9572122571599235861)
XLA Ops:
  0.0 105.9 %shard_map.118 = bf16[512,768]{1,0:T(8,128)(2,1)S(1)} custom-call(bf16[512,768]{1,0:T(8,128)(2,1)} %tokens_in.1, f32[2,768]{1,0:T(2,128)} %gain_in.1, f32[2,1056,768]{2,1,0:T(8,128)} %bitcast.4, f32[2,1056]{1,0:T(2,128)} %gs_in.1, f32[2,1056,768]{2,1,0:T(8,128)} %bitcast.5, f32[2,1056]{1,0:T(2,128)} %vs_in.1, f32[3,2,1056]{2,1,0:T(2,128)} %bitcast.6, ...), custom_call_target="tpu_custom_call" | custom-call | tf_op jit(solution)/shard_map/pallas_call | solution.py:604
  105.9 0.9 copy.14

commit v4 on v3

--- a/solution.py
+++ b/solution.py
@@ -115,18 +115,18 @@
     ]
 
     barrier = pltpu.get_barrier_semaphore()
+    @pl.when(z > 0)
+    def _():
+        pl.semaphore_signal(barrier, inc=1, device_id={"ra": z - 1}, device_id_type=MESH)
+
+    @pl.when(z < R - 1)
+    def _():
+        pl.semaphore_signal(barrier, inc=1, device_id={"ra": z + 1}, device_id_type=MESH)
+
     for k in range(1, N):
         pl.semaphore_signal(
             barrier, inc=1, device_id={"cb": lax.rem(me + k, N)}, device_id_type=MESH
         )
-
-    @pl.when(z > 0)
-    def _():
-        pl.semaphore_signal(barrier, inc=1, device_id={"ra": z - 1}, device_id_type=MESH)
-
-    @pl.when(z < R - 1)
-    def _():
-        pl.semaphore_signal(barrier, inc=1, device_id={"ra": z + 1}, device_id_type=MESH)
 
     C = first_sem.shape[1]
     step = full // C
@@ -263,9 +263,6 @@
     cast_rest(0)
     keep_tail(0, times_up(normed, 0, 2 * full, 2 * full + LANES), squares)
 
-    set_par()
-    for k in range(2):
-        fetch(1, k)
     expected = N - 1 + jnp.where(z > 0, 1, 0) + jnp.where(z < R - 1, 1, 0)
     pl.semaphore_wait(barrier, expected)
 
@@ -517,6 +514,12 @@
         when_item(t - FIRST - HOP * (R - 1 - z), lambda l, i, q: chain(1, l, q))
         when_item(t - at_gather, gathered, outer)
         when_far(t - far_gather, gathered)
+        @pl.when(t == 1)
+        def _():
+            set_par()
+            for k in range(2):
+                fetch(1, k)
+
         pl.when(t < n)(lambda: take(t))
         when_item(t, products)
 

time: 107 us -> 107 us (level)
  no operation moved by 1% of the time
where the time goes in v4:
time: 107 us
  Pallas kernels  106 us (99%)
    pallas_call x1, Pallas kernels, shards(): pl.pallas_call(functools.partial(kernel, cfg), out_shape=pltpu.VMEM((T, D...  106 us

profile of v4, /device:TPU:0, one launch (start us, length us, event | category | flops | bytes accessed | tf_op | source)
XLA Modules:
  0.0 106.6 jit_solution(16655470092380151823)
XLA Ops:
  0.0 105.7 %shard_map.118 = bf16[512,768]{1,0:T(8,128)(2,1)S(1)} custom-call(bf16[512,768]{1,0:T(8,128)(2,1)} %tokens_in.1, f32[2,768]{1,0:T(2,128)} %gain_in.1, f32[2,1056,768]{2,1,0:T(8,128)} %bitcast.4, f32[2,1056]{1,0:T(2,128)} %gs_in.1, f32[2,1056,768]{2,1,0:T(8,128)} %bitcast.5, f32[2,1056]{1,0:T(2,128)} %vs_in.1, f32[3,2,1056]{2,1,0:T(2,128)} %bitcast.6, ...), custom_call_target="tpu_custom_call" | custom-call | tf_op jit(solution)/shard_map/pallas_call | solution.py:607
  105.7 0.9 copy.14
